TPU v7x, 512 devices: a whole 4x8x8 slice. The times are simulated.
512 devices in a mesh: sp: 32 (over z, x), tp: 16 (over y, core).
Axes of the slice: x: 4, y: 8, z: 8, core: 2. Of those that a mesh axis runs over, the one named last changes fastest.
Arguments:
- queries: bfloat16 [12288, 1024], P('sp', 'tp'), may hold values from -6 to 6
- keys: bfloat16 [12288, 1024], P('sp', 'tp'), may hold values from -6 to 6
- values: bfloat16 [12288, 1024], P('sp', 'tp'), may hold values from -6 to 6
- log_cum: float32 [16, 12288], P('tp'), as said below
- residual: bfloat16 [12288, 2048], P('sp', 'tp'), may hold values from -6 to 6
- out_gain: float32 [1024], replicated, may hold values from 0.1 to 1.9
- w_out: bfloat16 [1024, 2048], P(None, 'tp'), may hold values from -0.1875 to 0.1875
- ffn_gain: float32 [2048], replicated, may hold values from 0.1 to 1.9
- routes: int32 [12288, 2], P('sp'), may hold values from 0 to 63, all different within a row; in each aligned block of 384 rows (0 to 383, 384 to 767, ...) at most 24 rows name the same one
- route_weight: float32 [12288, 2], P('sp'), may hold values from 0.25 to 2
- sh_gate: bfloat16 [2048, 512], P(None, 'tp'), may hold values from -0.125 to 0.125
- sh_up: bfloat16 [2048, 512], P(None, 'tp'), may hold values from -0.125 to 0.125
- sh_down: bfloat16 [512, 2048], P(None, 'tp'), may hold values from -0.25 to 0.25
- exp_gate: bfloat16 [64, 2048, 512], P('sp', None, 'tp'), may hold values from -0.125 to 0.125
- exp_up: bfloat16 [64, 2048, 512], P('sp', None, 'tp'), may hold values from -0.125 to 0.125
- exp_down: bfloat16 [64, 512, 2048], P('sp', None, 'tp'), may hold values from -0.25 to 0.25
Outputs:
- result: bfloat16 [12288, 2048], P('sp', 'tp')
Inputs may be any that keep to these rules, and one draw needn't show every extreme that they name: `routes`: in each aligned block of 384 rows no expert is named by more than 24 rows, a bound that some block reaches. `log_cum`: never rises along positions.
All inputs are finite; a program needn't handle non-finite values.
Results may differ from a plain program's by a relative error of at most 0.0095.
Values may be sent and summed in bfloat16 or wider, within the bound.
No kernel may reach another device: no remote copies, remote signals or barrier semaphores. Data moves between devices by JAX's collectives and lax.ppermute only.
A program may use at most 64 MiB of HBM per device.

v0:
```python
import jax
import jax.numpy as jnp
from jax import lax
from jax.sharding import PartitionSpec as P

EPS = 1e-06


def side_by_side(arrays, axis, dim, along):
    ends, at = ([], 0)
    for a in arrays[:-1]:
        at += a.shape[along]
        ends.append(at)
    both = jnp.concatenate(arrays, axis=along)
    return tuple(jnp.split(lax.all_gather(both, axis, axis=dim, tiled=True), ends, axis=along))


def copy_for_each(value, axis):
    copies = jnp.broadcast_to(value, (lax.axis_size(axis), *value.shape))
    return lax.all_to_all(copies, axis, split_axis=0, concat_axis=0, tiled=True)


def joined_along(pieces, dim):
    shape = list(pieces.shape[1:])
    shape[dim] *= pieces.shape[0]
    return jnp.moveaxis(pieces, 0, dim).reshape(shape)


def collect(value, axis, dim):
    pieces = copy_for_each(value, axis)
    return joined_along(pieces, dim)


def rms_scaled(matrix, gain):
    floats = matrix.astype(jnp.float32)
    inverse = lax.rsqrt(jnp.mean(floats * floats, axis=-1, keepdims=True) + EPS)
    return (floats * inverse * gain).astype(jnp.bfloat16)


def gated_hidden(gate, upward):
    return (jax.nn.silu(gate) * upward).astype(jnp.bfloat16)


def per_device(
    queries,
    keys,
    values,
    log_cum,
    residual,
    out_gain,
    w_out,
    ffn_gain,
    routes,
    route_weight,
    sh_gate,
    sh_up,
    sh_down,
    exp_gate,
    exp_up,
    exp_down,
):
    row_count = queries.shape[0]
    heads_here = log_cum.shape[0]
    head_size = queries.shape[1] // heads_here
    scale = head_size ** (-0.5)
    offset = lax.axis_index("sp") * row_count
    query_heads = queries.reshape(row_count, heads_here, head_size)
    query_pos = offset + lax.iota(jnp.int32, row_count)
    cum_query = lax.dynamic_slice_in_dim(log_cum, offset, row_count, 1)
    best = jnp.full((heads_here, row_count), -1e30, jnp.float32)
    key_piece, value_piece = side_by_side((keys, values), "sp", 0, 1)
    count = key_piece.shape[0]
    key_heads = key_piece.reshape(count, heads_here, head_size)
    value_heads = value_piece.reshape(count, heads_here, head_size)
    causal = lax.iota(jnp.int32, count)[None, :] <= query_pos[:, None]
    score = (
        jnp.einsum("qhd,khd->hqk", query_heads, key_heads, preferred_element_type=jnp.float32)
        * scale
    )
    score = jnp.where(causal[None], score + cum_query[:, :, None] - log_cum[:, None, :], -1e30)
    new_best = jnp.maximum(best, jnp.max(score, axis=2))
    weight = jnp.where(causal[None], jnp.exp(score - new_best[:, :, None]), 0.0)
    running_sum = jnp.sum(weight, axis=2)
    weighted = jnp.einsum(
        "hqk,khd->hqd", weight.astype(jnp.bfloat16), value_heads, preferred_element_type=jnp.float32
    )
    best, running_sum, weighted = (new_best, running_sum, weighted)
    head_out = (
        jnp.transpose(weighted / running_sum[:, :, None], (1, 0, 2))
        .reshape(row_count, heads_here * head_size)
        .astype(jnp.bfloat16)
    )
    all_heads = lax.all_gather(head_out, "tp", axis=1, tiled=True)
    mixed = rms_scaled(all_heads, out_gain)
    attended = jnp.dot(mixed, w_out, preferred_element_type=jnp.float32)
    updated = (residual.astype(jnp.float32) + attended).astype(jnp.bfloat16)
    full_rows = collect(updated, "tp", 1)
    normed = rms_scaled(full_rows, ffn_gain)
    width = normed.shape[1]
    shared_part = gated_hidden(
        jnp.dot(normed, sh_gate, preferred_element_type=jnp.float32),
        jnp.dot(normed, sh_up, preferred_element_type=jnp.float32),
    )
    shared_all = lax.all_gather(shared_part, "tp", axis=1, tiled=True)
    shared_out = jnp.dot(shared_all, sh_down, preferred_element_type=jnp.float32)
    top_count = routes.shape[1]
    expert_local = exp_gate.shape[0]
    sp_count = lax.axis_size("sp")
    tp_count = lax.axis_size("tp")
    expert_count = expert_local * sp_count
    capacity = 2 * row_count * top_count // expert_count
    assigned = routes.reshape(-1)
    onehot = (assigned[:, None] == lax.iota(jnp.int32, expert_count)[None, :]).astype(jnp.int32)
    slot_rank = jnp.sum((jnp.cumsum(onehot, axis=0) - 1) * onehot, axis=1)
    slot = assigned * capacity + slot_rank
    owner_row = lax.iota(jnp.int32, assigned.shape[0]) // top_count
    table = jnp.full((expert_count * capacity,), row_count, jnp.int32).at[slot].set(owner_row)
    padded = jnp.concatenate([normed, jnp.zeros((1, width), jnp.bfloat16)], axis=0)
    outgoing = padded[table].reshape(sp_count, expert_local * capacity, width)
    share = expert_local * capacity // tp_count
    portion = lax.dynamic_slice_in_dim(outgoing, lax.axis_index("tp") * share, share, 1)
    landed = lax.all_to_all(portion, "sp", split_axis=0, concat_axis=0, tiled=True)
    arrived = lax.all_gather(landed, "tp", axis=1, tiled=True)
    arrived = arrived.reshape(sp_count, expert_local, capacity, width)
    gate_part = jnp.einsum("secd,edf->secf", arrived, exp_gate, preferred_element_type=jnp.float32)
    up_part = jnp.einsum("secd,edf->secf", arrived, exp_up, preferred_element_type=jnp.float32)
    hidden = gated_hidden(gate_part, up_part)
    hidden_all = lax.all_gather(hidden, "tp", axis=3, tiled=True)
    expert_out = jnp.einsum(
        "secf,efd->secd", hidden_all, exp_down, preferred_element_type=jnp.float32
    ).astype(jnp.bfloat16)
    returned = lax.all_to_all(expert_out, "sp", split_axis=0, concat_axis=0, tiled=True)
    returned = returned.reshape(expert_count * capacity, returned.shape[3])
    picked = returned[slot].astype(jnp.float32) * route_weight.reshape(-1)[:, None]
    routed = jnp.sum(picked.reshape(row_count, top_count, picked.shape[1]), axis=1)
    return (updated.astype(jnp.float32) + shared_out + routed).astype(jnp.bfloat16)


def solution(mesh):
    in_specs = (
        P("sp", "tp"),
        P("sp", "tp"),
        P("sp", "tp"),
        P("tp", None),
        P("sp", "tp"),
        P(),
        P(None, "tp"),
        P(),
        P("sp", None),
        P("sp", None),
        P(None, "tp"),
        P(None, "tp"),
        P(None, "tp"),
        P("sp", None, "tp"),
        P("sp", None, "tp"),
        P("sp", None, "tp"),
    )
    out_specs = P("sp", "tp")
    return jax.shard_map(
        per_device, mesh=mesh, in_specs=in_specs, out_specs=out_specs, check_vma=False
    )
```

profile of v0, /device:TPU:1, one launch (start us, length us, event | category | flops | bytes accessed | tf_op | source)
XLA Modules:
  0.0 371.9 jit_solution(12435414797633586448)
XLA Ops:
  6.5 1.5 pad_maximum_fusion
  8.1 0.7 dynamic-slice_reduce_fusion
  8.8 88.6 %all-gather.4.cloned.1.call-done = bf16[12288,128]{0,1:T(8,128)(2,1)} async-done(((bf16[384,128]{0,1:T(8,128)(2,1)}), bf16[12288,128]{0,1:T(8,128)(2,1)}) %all-gather.4.cloned.1.call-update) | async-done | bytes 3145744 | tf_op jit(solution)/shard_map/all_gather | solution.py:15
  97.4 8.4 %fusion.60 = (f32[384]{0:T(512)S(1)}, f32[384,12288]{0,1:T(8,128)S(1)}) fusion(f32[12288]{0:T(1024)} %bitcast.74, f32[384]{0:T(512)S(1)} %dynamic-slice_reduce_fusion, bf16[384,64]{0,1:T(8,128)(2,1)} %param.16, bf16[12288,128]{0,1:T(8,128)(2,1)} %all-gather.4.cloned.1.call-done, s32[384]{0:T(512)S(1)} %iota_add_fusion), kind=kOutput, calls=%fused_computation.79 | convolution fusion | flops 632290944 | bytes 20550144 | tf_op jit(solution)/shard_map/qhd,khd->hqk/dot_general | solution.py:77
  105.9 4.8 %fusion = f32[384]{0:T(512)S(1)} fusion(f32[384,12288]{0,1:T(8,128)S(1)} %get-tuple-element.6, f32[384]{0:T(512)S(1)} %broadcast_maximum_fusion, s32[384]{0:T(512)S(1)} %iota_add_fusion), kind=kLoop, calls=%fused_computation.6 | loop fusion | flops 18873984 | bytes 18878976 | tf_op jit(solution)/shard_map/reduce_sum | solution.py:83
  110.6 3.7 %fusion.38 = bf16[384,64]{0,1:T(8,128)(2,1)S(1)} fusion(f32[384,12288]{0,1:T(8,128)S(1)} %get-tuple-element.6, f32[384]{0:T(512)S(1)} %broadcast_maximum_fusion, s32[384]{0:T(512)S(1)} %iota_add_fusion, bf16[12288,128]{0,1:T(8,128)(2,1)S(1)} %copy-done.6, f32[384]{0:T(512)S(1)} %fusion), kind=kOutput, calls=%fused_computation.40 | convolution fusion | flops 622903296 | bytes 20502528 | tf_op jit(solution)/shard_map/hqk,khd->hqd/dot_general | solution.py:84
  114.4 23.0 %all_gather.16 = bf16[384,1024]{0,1:T(8,128)(2,1)S(1)} all-gather(bf16[384,64]{0,1:T(8,128)(2,1)S(1)} %fusion.38), channel_id=1, replica_groups=mesh['sp'=32,'tp'=16] {'tp'}, dimensions={1}, use_global_device_ids=true | all-gather | bytes 835584 | tf_op jit(solution)/shard_map/all_gather | solution.py:93
  137.7 0.6 fusion.30
  138.3 1.5 broadcast_in_dim.18
  139.8 4.7 %all-to-all-start = ((bf16[16,384,128]{2,1,0:T(8,128)(2,1)}), bf16[16,384,128]{2,1,0:T(8,128)(2,1)S(1)}, u32[]{:S(2)}, u32[]{:S(2)}) async-start(bf16[16,384,128]{2,1,0:T(8,128)(2,1)} %broadcast_in_dim.18), calls=%async_computation | async-start | bytes 3145728 | tf_op jit(solution)/shard_map/all_to_all | solution.py:20
  145.0 1.8 reduce-window.6
  147.6 3.4 scatter_custom_fusion
  151.0 32.0 %all-to-all-done = bf16[16,384,128]{2,1,0:T(8,128)(2,1)S(1)} async-done(((bf16[16,384,128]{2,1,0:T(8,128)(2,1)}), bf16[16,384,128]{2,1,0:T(8,128)(2,1)S(1)}, u32[]{:S(2)}, u32[]{:S(2)}) %all-to-all-start) | async-done | bytes 1572896 | tf_op jit(solution)/shard_map/all_to_all | solution.py:20
  184.0 7.1 %gather_fusion = bf16[1536,2048]{1,0:T(8,128)(2,1)} fusion(bf16[385,2048]{1,0:T(8,128)(2,1)S(1)} %concatenate.7, s32[2048]{0:T(1024)S(1)} %pad_clamp_fusion), kind=kCustom, calls=%fused_computation | custom fusion | bytes 12589056 | tf_op jit(solution)/shard_map/gather | solution.py:119
  191.1 2.0 constant_dynamic-slice_fusion
  193.1 24.7 %all_to_all.15 = bf16[32,3,2048]{2,1,0:T(4,128)(2,1)S(1)} all-to-all(bf16[32,3,2048]{2,1,0:T(4,128)(2,1)S(1)} %constant_dynamic-slice_fusion), channel_id=1, replica_groups=mesh['sp'=32,'tp'=16] {'sp'}, dimensions={0} | all-to-all | bytes 786432 | tf_op jit(solution)/shard_map/all_to_all | solution.py:122
  217.8 1.1 copy.43
  218.9 42.5 %all-gather.6.cloned.1.call-done = bf16[32,48,2048]{2,0,1:T(8,128)(2,1)} async-done(((bf16[32,3,2048]{2,0,1:T(8,128)(2,1)}), bf16[32,48,2048]{2,0,1:T(8,128)(2,1)}) %all-gather.6.cloned.1.call-update) | async-done | bytes 6291472 | tf_op jit(solution)/shard_map/all_gather | solution.py:123
  261.4 7.5 %fusion.16 = f32[32,2,24,32]{3,2,0,1:T(8,128)S(1)} fusion(bf16[32,2,24,2048]{3,0,2,1:T(8,128)(2,1)} %bitcast.75, bf16[2,2048,32]{1,2,0:T(8,128)(2,1)} %param.29), kind=kOutput, calls=%fused_computation.26 | convolution fusion | flops 201326592 | bytes 6750208 | tf_op jit(solution)/shard_map/secd,edf->secf/dot_general | solution.py:125
  269.0 4.7 %fusion.25 = bf16[32,2,24,32]{3,2,0,1:T(8,128)(2,1)S(1)} fusion(bf16[32,2,24,2048]{3,0,2,1:T(8,128)(2,1)S(1)} %bitcast.76, f32[32,2,24,32]{3,2,0,1:T(8,128)S(1)} %fusion.16, bf16[2,2048,32]{1,2,0:T(8,128)(2,1)S(1)} %copy-done.8), kind=kOutput, calls=%fused_computation.30 | convolution fusion | flops 201621504 | bytes 6848512 | tf_op jit(solution)/shard_map/secd,edf->secf/dot_general | solution.py:126
  273.6 1.2 copy.47
  274.9 47.6 %all-gather.8.cloned.1.call-done = bf16[32,2,24,512]{0,2,1,3:T(8,128)(2,1)} async-done(((bf16[32,2,24,32]{0,2,1,3:T(8,128)(2,1)}), bf16[32,2,24,512]{0,2,1,3:T(8,128)(2,1)}) %all-gather.8.cloned.1.call-update) | async-done | bytes 1572880 | tf_op jit(solution)/shard_map/all_gather | solution.py:128
  322.5 7.4 %copy.48 = bf16[32,2,24,512]{3,2,0,1:T(8,128)(2,1)S(1)} copy(bf16[32,2,24,512]{0,2,1,3:T(8,128)(2,1)} %all-gather.8.cloned.1.call-done) | data formatting | bytes 3145728 | tf_op jit(solution)/shard_map/all_gather | solution.py:128
  329.9 0.6 fusion.28
  330.5 0.8 copy.49
  331.3 9.9 %all-to-all-start.2 = ((bf16[32,2,24,128]{3,2,1,0:T(8,128)(2,1)}), bf16[32,2,24,128]{3,2,1,0:T(8,128)(2,1)S(1)}, u32[]{:S(2)}, u32[]{:S(2)}) async-start(bf16[32,2,24,128]{3,2,1,0:T(8,128)(2,1)} %copy.49), calls=%async_computation.2 | async-start | bytes 786432 | tf_op jit(solution)/shard_map/all_to_all | solution.py:132
  341.4 1.5 fusion.61
  342.9 1.5 fusion.32
  344.4 17.5 %all_gather.17 = bf16[384,512]{0,1:T(8,128)(2,1)S(1)} all-gather(bf16[384,32]{0,1:T(8,128)(2,1)S(1)} %fusion.32), channel_id=1, replica_groups=mesh['sp'=32,'tp'=16] {'tp'}, dimensions={1}, use_global_device_ids=true | all-gather | bytes 417792 | tf_op jit(solution)/shard_map/all_gather | solution.py:104
  361.9 1.9 gather_fusion.1
  363.8 0.6 fusion.46
  364.4 1.0 fusion.31
  (53 shorter events, 2.8 us)
Async XLA Ops:
  6.5 323.4 %copy-start = (bf16[2,512,128]{2,1,0:T(8,128)(2,1)S(1)}, bf16[2,512,128]{2,1,0:T(8,128)(2,1)}, u32[]{:S(2)}) copy-start(bf16[2,512,128]{2,1,0:T(8,128)(2,1)} %param.31) | copy-start | bytes 786436
  6.5 90.9 %all-gather.4.cloned.1.call-start = ((), (), s32[]{:S(2)}) async-start(), calls=%async_computation.3 | async-start | bytes 3244032 | tf_op jit(solution)/shard_map/all_gather | solution.py:15
  105.8 4.8 %copy-start.6 = (bf16[12288,128]{0,1:T(8,128)(2,1)S(1)}, bf16[12288,128]{0,1:T(8,128)(2,1)}, u32[]{:S(2)}) copy-start(bf16[12288,128]{0,1:T(8,128)(2,1)} %all-gather.4.cloned.1.call-done) | copy-start | bytes 9437188
  110.6 27.1 %copy-start.7 = (bf16[1024,128]{1,0:T(8,128)(2,1)S(1)}, bf16[1024,128]{1,0:T(8,128)(2,1)}, u32[]{:S(2)}) copy-start(bf16[1024,128]{1,0:T(8,128)(2,1)} %param.22) | copy-start | bytes 786436
  110.6 27.0 %copy-start.9 = (bf16[384,128]{1,0:T(8,128)(2,1)S(1)}, bf16[384,128]{1,0:T(8,128)(2,1)}, u32[]{:S(2)}) copy-start(bf16[384,128]{1,0:T(8,128)(2,1)} %param.20) | copy-start | bytes 294916
  110.6 27.0 %copy-start.10 = (f32[1024]{0:T(1024)S(1)}, f32[1024]{0:T(1024)}, u32[]{:S(2)}) copy-start(f32[1024]{0:T(1024)} %param.21) | copy-start | bytes 12292
  114.4 30.1 %copy-start.2 = (s32[384,2]{0,1:T(2,128)S(1)}, s32[384,2]{0,1:T(2,128)}, u32[]{:S(2)}) copy-start(s32[384,2]{0,1:T(2,128)} %param.24) | copy-start | bytes 9220
  137.7 45.7 %copy-start.3 = (f32[2048]{0:T(1024)S(1)}, f32[2048]{0:T(1024)}, u32[]{:S(2)}) copy-start(f32[2048]{0:T(1024)} %param.23) | copy-start | bytes 24580
  139.8 43.2 %all-to-all-start = ((bf16[16,384,128]{2,1,0:T(8,128)(2,1)}), bf16[16,384,128]{2,1,0:T(8,128)(2,1)S(1)}, u32[]{:S(2)}, u32[]{:S(2)}) async-start(bf16[16,384,128]{2,1,0:T(8,128)(2,1)} %broadcast_in_dim.18), calls=%async_computation | async-start | bytes 3145728 | tf_op jit(solution)/shard_map/all_to_all | solution.py:20
  144.5 116.9 %all-gather.6.cloned.1.call-start = ((), (), s32[]{:S(2)}) async-start(), calls=%async_computation.4 | async-start | bytes 6684672 | tf_op jit(solution)/shard_map/all_gather | solution.py:123
  218.8 103.6 %all-gather.8.cloned.1.call-start = ((), (), s32[]{:S(2)}) async-start(), calls=%async_computation.5 | async-start | bytes 6684672 | tf_op jit(solution)/shard_map/all_gather | solution.py:128
  261.4 7.5 %copy-start.5 = (bf16[32,48,2048]{2,0,1:T(8,128)(2,1)S(1)}, bf16[32,48,2048]{2,0,1:T(8,128)(2,1)}, u32[]{:S(2)}) copy-start(bf16[32,48,2048]{2,0,1:T(8,128)(2,1)} %all-gather.6.cloned.1.call-done) | copy-start | bytes 18874372
  261.4 7.5 %copy-start.8 = (bf16[2,2048,32]{1,2,0:T(8,128)(2,1)S(1)}, bf16[2,2048,32]{1,2,0:T(8,128)(2,1)}, u32[]{:S(2)}) copy-start(bf16[2,2048,32]{1,2,0:T(8,128)(2,1)} %param.30) | copy-start | bytes 786436
  274.9 66.4 %copy-start.4 = (f32[384,2]{0,1:T(2,128)S(1)}, f32[384,2]{0,1:T(2,128)}, u32[]{:S(2)}) copy-start(f32[384,2]{0,1:T(2,128)} %param.25) | copy-start | bytes 9220
  330.5 33.8 %copy-start.1 = (bf16[512,128]{1,0:T(8,128)(2,1)S(1)}, bf16[512,128]{1,0:T(8,128)(2,1)}, u32[]{:S(2)}) copy-start(bf16[512,128]{1,0:T(8,128)(2,1)} %param.28) | copy-start | bytes 393220
  331.3 30.6 %all-to-all-start.2 = ((bf16[32,2,24,128]{3,2,1,0:T(8,128)(2,1)}), bf16[32,2,24,128]{3,2,1,0:T(8,128)(2,1)S(1)}, u32[]{:S(2)}, u32[]{:S(2)}) async-start(bf16[32,2,24,128]{3,2,1,0:T(8,128)(2,1)} %copy.49), calls=%async_computation.2 | async-start | bytes 786432 | tf_op jit(solution)/shard_map/all_to_all | solution.py:132
Sparse Core Ops, SparseCore 0:
  10.4 86.9 all-gather.3
  219.0 42.3 all-gather.5
  275.0 47.4 all-gather.7
where the time goes:
time: 372 us
  waiting for transfers between devices  211 us (57%)
  blocking collectives  65.2 us (18%)
  matrix products  29.4 us (8%)
  local copies, waits for them, and re-layouts  28.4 us (8%)
  starting transfers between devices  14.6 us (4%)
  between operations  13.5 us (4%)
  other arithmetic  9.93 us (3%)
    all_gather x1, waiting for transfers between devices, side_by_side(): lax.all_gather(both, axis, axis=dim, tiled=True)  88.6 us
    all_gather x1, waiting for transfers between devices, per_device(): hidden_all = lax.all_gather(hidden, 'tp', axis=3, tiled=True)  47.6 us
    all_gather x1, waiting for transfers between devices, per_device(): arrived = lax.all_gather(landed, 'tp', axis=1, tiled=True)  42.5 us
    all_to_all x1, waiting for transfers between devices, copy_for_each(): return lax.all_to_all(copies, axis, split_axis=0, concat_axis=0, tiled=True)  32 us
    all_to_all x1, blocking collectives, per_device(): lax.all_to_all(portion, 'sp', split_axis=0, concat_axis=0, tiled=True)  24.7 us
    all_gather x1, blocking collectives, per_device(): all_heads = lax.all_gather(head_out, 'tp', axis=1, tiled=True)  23 us
    all_gather x1, blocking collectives, per_device(): shared_all = lax.all_gather(shared_part, 'tp', axis=1, tiled=True)  17.5 us
    all_to_all x1, starting transfers between devices, per_device(): lax.all_to_all(expert_out, 'sp', split_axis=0, concat_axis=0, tiled=True)  9.9 us
  transfers between devices with their start and end apart: 5, of which 4 were waited for; matrix products, arithmetic and copies ran while one was open for 3% of the time, Pallas kernels for 0%

commit v1 on v0

--- a/solution.py
+++ b/solution.py
@@ -90,7 +90,7 @@
         .reshape(row_count, heads_here * head_size)
         .astype(jnp.bfloat16)
     )
-    all_heads = lax.all_gather(head_out, "tp", axis=1, tiled=True)
+    all_heads = jnp.concatenate(lax.all_gather(head_out, "tp"), axis=1)
     mixed = rms_scaled(all_heads, out_gain)
     attended = jnp.dot(mixed, w_out, preferred_element_type=jnp.float32)
     updated = (residual.astype(jnp.float32) + attended).astype(jnp.bfloat16)

time: 372 us -> 373 us (level)
  no operation moved by 1% of the time
where the time goes in v1:
time: 373 us; the launch traced here: 372 us
  waiting for transfers between devices  211 us (57%)
  blocking collectives  65.2 us (17%)
  matrix products  29.2 us (8%)
  local copies, waits for them, and re-layouts  29.1 us (8%)
  starting transfers between devices  14.6 us (4%)
  between operations  13.5 us (4%)
  other arithmetic  10.2 us (3%)
    all_gather x1, waiting for transfers between devices, side_by_side(): lax.all_gather(both, axis, axis=dim, tiled=True)  88.6 us
    all_gather x1, waiting for transfers between devices, per_device(): hidden_all = lax.all_gather(hidden, 'tp', axis=3, tiled=True)  47.6 us
    all_gather x1, waiting for transfers between devices, per_device(): arrived = lax.all_gather(landed, 'tp', axis=1, tiled=True)  42.5 us
    all_to_all x1, waiting for transfers between devices, copy_for_each(): return lax.all_to_all(copies, axis, split_axis=0, concat_axis=0, tiled=True)  31.8 us
    all_to_all x1, blocking collectives, per_device(): lax.all_to_all(portion, 'sp', split_axis=0, concat_axis=0, tiled=True)  24.7 us
    all_gather x1, blocking collectives, per_device(): all_heads = jnp.concatenate(lax.all_gather(head_out, 'tp'), axis=1)  23 us
    all_gather x1, blocking collectives, per_device(): shared_all = lax.all_gather(shared_part, 'tp', axis=1, tiled=True)  17.5 us
    all_to_all x1, starting transfers between devices, per_device(): lax.all_to_all(expert_out, 'sp', split_axis=0, concat_axis=0, tiled=True)  9.9 us
  transfers between devices with their start and end apart: 5, of which 4 were waited for; matrix products, arithmetic and copies ran while one was open for 3% of the time, Pallas kernels for 0%

profile of v1, /device:TPU:1, one launch (start us, length us, event | category | flops | bytes accessed | tf_op | source)
XLA Modules:
  0.0 372.4 jit_solution(17976360601174268218)
XLA Ops:
  6.5 1.5 pad_maximum_fusion
  8.1 0.7 dynamic-slice_reduce_fusion
  8.8 88.6 %all-gather.5.cloned.1.call-done = bf16[12288,128]{0,1:T(8,128)(2,1)} async-done(((bf16[384,128]{0,1:T(8,128)(2,1)}), bf16[12288,128]{0,1:T(8,128)(2,1)}) %all-gather.5.cloned.1.call-update) | async-done | bytes 3145744 | tf_op jit(solution)/shard_map/all_gather | solution.py:15
  97.4 8.4 %fusion.57 = (f32[384]{0:T(512)S(1)}, f32[384,12288]{0,1:T(8,128)S(1)}) fusion(f32[12288]{0:T(1024)} %bitcast.97, f32[384]{0:T(512)S(1)} %dynamic-slice_reduce_fusion, bf16[384,64]{0,1:T(8,128)(2,1)} %param.16, bf16[12288,128]{0,1:T(8,128)(2,1)} %all-gather.5.cloned.1.call-done, s32[384]{0:T(512)S(1)} %iota_add_fusion), kind=kOutput, calls=%fused_computation.78 | convolution fusion | flops 632290944 | bytes 20550144 | tf_op jit(solution)/shard_map/qhd,khd->hqk/dot_general | solution.py:77
  105.9 4.8 %fusion = f32[384]{0:T(512)S(1)} fusion(f32[384,12288]{0,1:T(8,128)S(1)} %get-tuple-element.6, f32[384]{0:T(512)S(1)} %broadcast_maximum_fusion, s32[384]{0:T(512)S(1)} %iota_add_fusion), kind=kLoop, calls=%fused_computation.6 | loop fusion | flops 18873984 | bytes 18878976 | tf_op jit(solution)/shard_map/reduce_sum | solution.py:83
  110.6 3.7 %fusion.38 = bf16[384,64]{0,1:T(8,128)(2,1)S(1)} fusion(f32[384,12288]{0,1:T(8,128)S(1)} %get-tuple-element.6, f32[384]{0:T(512)S(1)} %broadcast_maximum_fusion, s32[384]{0:T(512)S(1)} %iota_add_fusion, bf16[12288,128]{0,1:T(8,128)(2,1)S(1)} %copy-done.9, f32[384]{0:T(512)S(1)} %fusion), kind=kOutput, calls=%fused_computation.41 | convolution fusion | flops 622903296 | bytes 20502528 | tf_op jit(solution)/shard_map/hqk,khd->hqd/dot_general | solution.py:84
  114.4 23.0 %all-gather = bf16[6144,64]{0,1:T(8,128)(2,1)S(1)} all-gather(bf16[384,64]{0,1:T(8,128)(2,1)S(1)} %fusion.38), channel_id=2, replica_groups=mesh['sp'=32,'tp'=16] {'tp'}, dimensions={0}, use_global_device_ids=true | all-gather | bytes 835584 | tf_op jit(solution)/shard_map/all_gather | solution.py:93
  138.9 1.5 broadcast_in_dim.18
  140.3 4.7 %all-to-all-start = ((bf16[16,384,128]{2,1,0:T(8,128)(2,1)}), bf16[16,384,128]{2,1,0:T(8,128)(2,1)S(1)}, u32[]{:S(2)}, u32[]{:S(2)}) async-start(bf16[16,384,128]{2,1,0:T(8,128)(2,1)} %broadcast_in_dim.18), calls=%async_computation | async-start | bytes 3145728 | tf_op jit(solution)/shard_map/all_to_all | solution.py:20
  145.5 1.8 reduce-window.6
  148.1 3.6 scatter_custom_fusion
  151.7 31.8 %all-to-all-done = bf16[16,384,128]{2,1,0:T(8,128)(2,1)S(1)} async-done(((bf16[16,384,128]{2,1,0:T(8,128)(2,1)}), bf16[16,384,128]{2,1,0:T(8,128)(2,1)S(1)}, u32[]{:S(2)}, u32[]{:S(2)}) %all-to-all-start) | async-done | bytes 1572896 | tf_op jit(solution)/shard_map/all_to_all | solution.py:20
  183.9 0.4 fusion.10
  184.6 7.1 %gather_fusion = bf16[1536,2048]{1,0:T(8,128)(2,1)} fusion(bf16[385,2048]{1,0:T(8,128)(2,1)S(1)} %concatenate.7, s32[2048]{0:T(1024)S(1)} %pad_clamp_fusion), kind=kCustom, calls=%fused_computation | custom fusion | bytes 12589056 | tf_op jit(solution)/shard_map/gather | solution.py:119
  191.7 2.0 constant_dynamic-slice_fusion
  193.6 24.7 %all_to_all.15 = bf16[32,3,2048]{2,1,0:T(4,128)(2,1)S(1)} all-to-all(bf16[32,3,2048]{2,1,0:T(4,128)(2,1)S(1)} %constant_dynamic-slice_fusion), channel_id=1, replica_groups=mesh['sp'=32,'tp'=16] {'sp'}, dimensions={0} | all-to-all | bytes 786432 | tf_op jit(solution)/shard_map/all_to_all | solution.py:122
  218.3 1.1 copy.46
  219.4 42.5 %all-gather.7.cloned.1.call-done = bf16[32,48,2048]{2,0,1:T(8,128)(2,1)} async-done(((bf16[32,3,2048]{2,0,1:T(8,128)(2,1)}), bf16[32,48,2048]{2,0,1:T(8,128)(2,1)}) %all-gather.7.cloned.1.call-update) | async-done | bytes 6291472 | tf_op jit(solution)/shard_map/all_gather | solution.py:123
  262.0 7.5 %fusion.16 = f32[32,2,24,32]{3,2,0,1:T(8,128)S(1)} fusion(bf16[32,2,24,2048]{3,0,2,1:T(8,128)(2,1)} %bitcast.98, bf16[2,2048,32]{1,2,0:T(8,128)(2,1)} %param.29), kind=kOutput, calls=%fused_computation.27 | convolution fusion | flops 201326592 | bytes 6750208 | tf_op jit(solution)/shard_map/secd,edf->secf/dot_general | solution.py:125
  269.5 4.7 %fusion.25 = bf16[32,2,24,32]{3,2,0,1:T(8,128)(2,1)S(1)} fusion(bf16[32,2,24,2048]{3,0,2,1:T(8,128)(2,1)S(1)} %bitcast.99, f32[32,2,24,32]{3,2,0,1:T(8,128)S(1)} %fusion.16, bf16[2,2048,32]{1,2,0:T(8,128)(2,1)S(1)} %copy-done.10), kind=kOutput, calls=%fused_computation.31 | convolution fusion | flops 201621504 | bytes 6848512 | tf_op jit(solution)/shard_map/secd,edf->secf/dot_general | solution.py:126
  274.2 1.2 copy.50
  275.4 47.6 %all-gather.9.cloned.1.call-done = bf16[32,2,24,512]{0,2,1,3:T(8,128)(2,1)} async-done(((bf16[32,2,24,32]{0,2,1,3:T(8,128)(2,1)}), bf16[32,2,24,512]{0,2,1,3:T(8,128)(2,1)}) %all-gather.9.cloned.1.call-update) | async-done | bytes 1572880 | tf_op jit(solution)/shard_map/all_gather | solution.py:128
  323.0 7.4 %copy.51 = bf16[32,2,24,512]{3,2,0,1:T(8,128)(2,1)S(1)} copy(bf16[32,2,24,512]{0,2,1,3:T(8,128)(2,1)} %all-gather.9.cloned.1.call-done) | data formatting | bytes 3145728 | tf_op jit(solution)/shard_map/all_gather | solution.py:128
  330.5 0.6 fusion.28
  331.1 0.8 copy.52
  331.9 9.9 %all-to-all-start.2 = ((bf16[32,2,24,128]{3,2,1,0:T(8,128)(2,1)}), bf16[32,2,24,128]{3,2,1,0:T(8,128)(2,1)S(1)}, u32[]{:S(2)}, u32[]{:S(2)}) async-start(bf16[32,2,24,128]{3,2,1,0:T(8,128)(2,1)} %copy.52), calls=%async_computation.2 | async-start | bytes 786432 | tf_op jit(solution)/shard_map/all_to_all | solution.py:132
  341.9 1.5 fusion.58
  343.4 1.5 fusion.32
  344.9 17.5 %all_gather.18 = bf16[384,512]{0,1:T(8,128)(2,1)S(1)} all-gather(bf16[384,32]{0,1:T(8,128)(2,1)S(1)} %fusion.32), channel_id=1, replica_groups=mesh['sp'=32,'tp'=16] {'tp'}, dimensions={1}, use_global_device_ids=true | all-gather | bytes 417792 | tf_op jit(solution)/shard_map/all_gather | solution.py:104
  362.4 1.9 gather_fusion.1
  364.3 0.6 fusion.43
  364.9 1.0 fusion.31
  (57 shorter events, 3.5 us)
Async XLA Ops:
  6.5 323.9 %copy-start = (bf16[2,512,128]{2,1,0:T(8,128)(2,1)S(1)}, bf16[2,512,128]{2,1,0:T(8,128)(2,1)}, u32[]{:S(2)}) copy-start(bf16[2,512,128]{2,1,0:T(8,128)(2,1)} %param.31) | copy-start | bytes 786436
  6.5 90.9 %all-gather.5.cloned.1.call-start = ((), (), s32[]{:S(2)}) async-start(), calls=%async_computation.3 | async-start | bytes 3244032 | tf_op jit(solution)/shard_map/all_gather | solution.py:15
  105.8 4.8 %copy-start.9 = (bf16[12288,128]{0,1:T(8,128)(2,1)S(1)}, bf16[12288,128]{0,1:T(8,128)(2,1)}, u32[]{:S(2)}) copy-start(bf16[12288,128]{0,1:T(8,128)(2,1)} %all-gather.5.cloned.1.call-done) | copy-start | bytes 9437188
  137.4 0.8 copy-start.6
  137.5 1.0 copy-start.1
  137.5 1.0 copy-start.3
  138.1 6.9 %copy-start.4 = (s32[384,2]{0,1:T(2,128)S(1)}, s32[384,2]{0,1:T(2,128)}, u32[]{:S(2)}) copy-start(s32[384,2]{0,1:T(2,128)} %param.24) | copy-start | bytes 9220
  138.5 45.5 %copy-start.5 = (f32[2048]{0:T(1024)S(1)}, f32[2048]{0:T(1024)}, u32[]{:S(2)}) copy-start(f32[2048]{0:T(1024)} %param.23) | copy-start | bytes 24580
  140.3 43.2 %all-to-all-start = ((bf16[16,384,128]{2,1,0:T(8,128)(2,1)}), bf16[16,384,128]{2,1,0:T(8,128)(2,1)S(1)}, u32[]{:S(2)}, u32[]{:S(2)}) async-start(bf16[16,384,128]{2,1,0:T(8,128)(2,1)} %broadcast_in_dim.18), calls=%async_computation | async-start | bytes 3145728 | tf_op jit(solution)/shard_map/all_to_all | solution.py:20
  145.0 116.9 %all-gather.7.cloned.1.call-start = ((), (), s32[]{:S(2)}) async-start(), calls=%async_computation.4 | async-start | bytes 6684672 | tf_op jit(solution)/shard_map/all_gather | solution.py:123
  219.4 103.6 %all-gather.9.cloned.1.call-start = ((), (), s32[]{:S(2)}) async-start(), calls=%async_computation.5 | async-start | bytes 6684672 | tf_op jit(solution)/shard_map/all_gather | solution.py:128
  261.9 7.5 %copy-start.8 = (bf16[32,48,2048]{2,0,1:T(8,128)(2,1)S(1)}, bf16[32,48,2048]{2,0,1:T(8,128)(2,1)}, u32[]{:S(2)}) copy-start(bf16[32,48,2048]{2,0,1:T(8,128)(2,1)} %all-gather.7.cloned.1.call-done) | copy-start | bytes 18874372
  262.0 7.5 %copy-start.10 = (bf16[2,2048,32]{1,2,0:T(8,128)(2,1)S(1)}, bf16[2,2048,32]{1,2,0:T(8,128)(2,1)}, u32[]{:S(2)}) copy-start(bf16[2,2048,32]{1,2,0:T(8,128)(2,1)} %param.30) | copy-start | bytes 786436
  275.4 66.4 %copy-start.7 = (f32[384,2]{0,1:T(2,128)S(1)}, f32[384,2]{0,1:T(2,128)}, u32[]{:S(2)}) copy-start(f32[384,2]{0,1:T(2,128)} %param.25) | copy-start | bytes 9220
  331.1 33.8 %copy-start.2 = (bf16[512,128]{1,0:T(8,128)(2,1)S(1)}, bf16[512,128]{1,0:T(8,128)(2,1)}, u32[]{:S(2)}) copy-start(bf16[512,128]{1,0:T(8,128)(2,1)} %param.28) | copy-start | bytes 393220
  331.9 30.6 %all-to-all-start.2 = ((bf16[32,2,24,128]{3,2,1,0:T(8,128)(2,1)}), bf16[32,2,24,128]{3,2,1,0:T(8,128)(2,1)S(1)}, u32[]{:S(2)}, u32[]{:S(2)}) async-start(bf16[32,2,24,128]{3,2,1,0:T(8,128)(2,1)} %copy.52), calls=%async_computation.2 | async-start | bytes 786432 | tf_op jit(solution)/shard_map/all_to_all | solution.py:132
Sparse Core Ops, SparseCore 0:
  10.4 86.9 all-gather.4
  219.5 42.3 all-gather.6
  275.5 47.4 all-gather.8
